TPU v7x, 32 devices: a whole 2x2x4 slice. The times are simulated.
32 devices in a mesh: ra: 8 (over z, x), cb: 4 (over y, core).
Axes of the slice: x: 2, y: 2, z: 4, core: 2. Of those that a mesh axis runs over, the one named last changes fastest.
Arguments:
- tokens: bfloat16 [64, 1024], P(None, 'ra'), may hold values from -14 to 14, as said below
- norm_gain_a: float32 [1024], P('ra'), may hold values from 0.1 to 1.9
- gate_weight_a: float32 [1024, 2816], P('ra', 'cb'), may hold values from -0.1875 to 0.1875
- up_weight_a: float32 [1024, 2816], P('ra', 'cb'), may hold values from -0.1875 to 0.1875
- down_weight_a: float32 [2816, 1024], P('cb', 'ra'), may hold values from -0.109375 to 0.109375
- norm_gain_b: float32 [1024], P('ra'), may hold values from 0.1 to 1.9
- gate_weight_b: float32 [1024, 2816], P('ra', 'cb'), may hold values from -0.1875 to 0.1875
- up_weight_b: float32 [1024, 2816], P('ra', 'cb'), may hold values from -0.1875 to 0.1875
- down_weight_b: float32 [2816, 1024], P('cb', 'ra'), may hold values from -0.109375 to 0.109375
Outputs:
- stream_out: bfloat16 [64, 1024], P(None, 'ra')
Inputs may be any that keep to these rules, and one draw needn't show every extreme that they name: Each feature of tokens carries its own scale, between about 0.3 and 3.3 across features; entries lie within -14 to 14.
All inputs are finite; a program needn't handle non-finite values.
Results may differ from a plain program's by a relative error of at most 0.008.
Values may be sent and summed in bfloat16 or wider, within the bound.
A program may use at most 64 MiB of HBM per device.

v0:
```python
import jax
import jax.numpy as jnp
from jax import lax
from jax.sharding import PartitionSpec as P

residual_weight = 0.5
epsilon = 1e-06


def hidden_of(normed, gate_cast, up_cast):
    gate_part = jnp.dot(normed, gate_cast, preferred_element_type=jnp.float32)
    up_part = jnp.dot(normed, up_cast, preferred_element_type=jnp.float32)
    gate_sum, up_sum = lax.psum((gate_part, up_part), "ra")
    return (jax.nn.silu(gate_sum) * up_sum).astype(jnp.bfloat16)


def normalize(as_float, square_total, gain):
    feature_count = as_float.shape[1] * lax.axis_size("ra")
    row_scale = lax.rsqrt(square_total / feature_count + epsilon)
    return (as_float * row_scale[:, None] * gain).astype(jnp.bfloat16)


def whole_sublayer(stream, gain, gate_weight, up_weight, down_weight):
    as_float = stream.astype(jnp.float32)
    square_total = lax.psum(jnp.sum(as_float * as_float, axis=1), "ra")
    normed = normalize(as_float, square_total, gain)
    hidden = hidden_of(normed, gate_weight.astype(jnp.bfloat16), up_weight.astype(jnp.bfloat16))
    branch_part = jnp.dot(
        hidden, down_weight.astype(jnp.bfloat16), preferred_element_type=jnp.float32
    )
    branch = lax.psum(branch_part, "cb")
    return (residual_weight * as_float + branch).astype(jnp.bfloat16)


def per_device(
    tokens,
    norm_gain_a,
    gate_weight_a,
    up_weight_a,
    down_weight_a,
    norm_gain_b,
    gate_weight_b,
    up_weight_b,
    down_weight_b,
):
    middle = whole_sublayer(tokens, norm_gain_a, gate_weight_a, up_weight_a, down_weight_a)
    return whole_sublayer(middle, norm_gain_b, gate_weight_b, up_weight_b, down_weight_b)


def solution(mesh):
    placed = (
        P(None, "ra"),
        P("ra"),
        P("ra", "cb"),
        P("ra", "cb"),
        P("cb", "ra"),
        P("ra"),
        P("ra", "cb"),
        P("ra", "cb"),
        P("cb", "ra"),
    )
    return jax.shard_map(
        per_device, mesh=mesh, in_specs=placed, out_specs=P(None, "ra"), check_vma=False
    )
```

profile of v0, /device:TPU:0, one launch (start us, length us, event | category | flops | bytes accessed | tf_op | source)
XLA Modules:
  0.0 224.8 jit_solution(7267552355934892765)
XLA Ops:
  6.5 0.0 copy-start.3
  6.5 0.0 copy-start
  6.5 0.0 all-reduce.7.cloned.1.call-start
  6.5 0.9 fusion.14
  7.4 23.2 %psum.56 = f32[64]{0:T(128)S(1)} all-reduce(f32[64]{0:T(128)S(1)} %fusion.14), channel_id=1, replica_groups=mesh['ra'=8,'cb'=4] {'ra'}, use_global_device_ids=true, to_apply=%region_1.0 | all-reduce | flops 64 | bytes 512 | tf_op jit(solution)/shard_map/psum | solution.py:25
  30.6 0.0 copy-done.3
  30.6 0.0 copy-start.4
  30.6 1.9 fusion.8
  32.5 0.0 copy-done
  32.5 0.0 copy-done.4
  32.5 0.0 copy-start.6
  32.5 0.9 fusion.10
  33.5 0.0 all-reduce.7.cloned.1.call-update
  33.5 0.0 all-reduce.5.cloned.1.call-start
  33.5 69.4 %all-reduce.7.cloned.1.call-done = (f32[64,704]{1,0:T(8,128)}, f32[64,704]{1,0:T(8,128)}) async-done(((f32[64,704]{1,0:T(8,128)}, f32[64,704]{1,0:T(8,128)}), (f32[64,704]{1,0:T(8,128)}, f32[64,704]{1,0:T(8,128)})) %all-reduce.7.cloned.1.call-update) | async-done | bytes 360464 | tf_op jit(solution)/shard_map/psum | solution.py:13
  103.0 0.0 copy-done.6
  103.0 0.0 copy-start.1
  103.0 0.0 copy-start.5
  103.0 1.3 fusion.6
  104.2 0.0 copy-start.2
  104.3 10.4 %psum.59 = f32[64,128]{1,0:T(8,128)S(1)} all-reduce(f32[64,128]{1,0:T(8,128)S(1)} %fusion.6), channel_id=1, replica_groups=mesh['ra'=8,'cb'=4] {'cb'}, use_global_device_ids=true, to_apply=%region_4.5 | all-reduce | flops 8192 | bytes 65536 | tf_op jit(solution)/shard_map/psum | solution.py:31
  114.7 0.1 fusion.19
  114.8 19.6 %psum.60 = f32[64]{0:T(128)S(1)} all-reduce(f32[64]{0:T(128)S(1)} %get-tuple-element.9), channel_id=1, replica_groups=mesh['ra'=8,'cb'=4] {'ra'}, use_global_device_ids=true, to_apply=%region_6.7 | all-reduce | flops 64 | bytes 512 | tf_op jit(solution)/shard_map/psum | solution.py:25
  134.4 0.0 copy-done.1
  134.4 0.0 copy-done.5
  134.4 0.9 fusion.2
  135.3 0.0 copy-done.2
  135.3 0.0 copy-start.7
  135.3 0.9 fusion.4
  136.3 0.0 all-reduce.5.cloned.1.call-update
  136.3 69.6 %all-reduce.5.cloned.1.call-done = (f32[64,704]{1,0:T(8,128)}, f32[64,704]{1,0:T(8,128)}) async-done(((f32[64,704]{1,0:T(8,128)}, f32[64,704]{1,0:T(8,128)}), (f32[64,704]{1,0:T(8,128)}, f32[64,704]{1,0:T(8,128)})) %all-reduce.5.cloned.1.call-update) | async-done | bytes 360464 | tf_op jit(solution)/shard_map/psum | solution.py:13
  205.9 0.0 copy-done.7
  205.9 1.2 fusion
  207.1 10.3 %psum.63 = f32[64,128]{1,0:T(8,128)S(1)} all-reduce(f32[64,128]{1,0:T(8,128)S(1)} %fusion), channel_id=1, replica_groups=mesh['ra'=8,'cb'=4] {'cb'}, use_global_device_ids=true, to_apply=%region_9.10 | all-reduce | flops 8192 | bytes 65536 | tf_op jit(solution)/shard_map/psum | solution.py:31
  217.4 0.6 fusion.18
  (2 shorter events, 0.0 us)
Async XLA Ops:
  6.5 24.1 %copy-start.3 = (bf16[64,128]{1,0:T(8,128)(2,1)S(1)}, bf16[64,128]{1,0:T(8,128)(2,1)}, u32[]{:S(2)}) copy-start(bf16[64,128]{1,0:T(8,128)(2,1)} %param.9) | copy-start | bytes 49156
  6.5 26.0 %copy-start = (f32[128,704]{0,1:T(8,128)S(1)}, f32[128,704]{0,1:T(8,128)}, u32[]{:S(2)}) copy-start(f32[128,704]{0,1:T(8,128)} %param.11) | copy-start | bytes 1081348
  6.5 96.4 %all-reduce.7.cloned.1.call-start = ((), (), s32[]{:S(2)}) async-start(), calls=%async_computation.1 | async-start | bytes 786432 | tf_op jit(solution)/shard_map/psum | solution.py:13
  30.6 1.9 copy-start.4
  32.5 70.4 %copy-start.6 = (f32[704,128]{1,0:T(8,128)S(1)}, f32[704,128]{1,0:T(8,128)}, u32[]{:S(2)}) copy-start(f32[704,128]{1,0:T(8,128)} %param.13) | copy-start | bytes 1081348
  33.5 172.4 %all-reduce.5.cloned.1.call-start = ((), (), s32[]{:S(2)}) async-start(), calls=%async_computation | async-start | bytes 786432 | tf_op jit(solution)/shard_map/psum | solution.py:13
  103.0 31.4 %copy-start.1 = (f32[128,704]{0,1:T(8,128)S(1)}, f32[128,704]{0,1:T(8,128)}, u32[]{:S(2)}) copy-start(f32[128,704]{0,1:T(8,128)} %param.16) | copy-start | bytes 1081348
  103.0 31.4 %copy-start.5 = (f32[128]{0:T(128)S(1)}, f32[128]{0:T(128)}, u32[]{:S(2)}) copy-start(f32[128]{0:T(128)} %param.14) | copy-start | bytes 1540
  104.2 31.1 %copy-start.2 = (f32[128,704]{0,1:T(8,128)S(1)}, f32[128,704]{0,1:T(8,128)}, u32[]{:S(2)}) copy-start(f32[128,704]{0,1:T(8,128)} %param.15) | copy-start | bytes 1081348
  135.3 70.5 %copy-start.7 = (f32[704,128]{1,0:T(8,128)S(1)}, f32[704,128]{1,0:T(8,128)}, u32[]{:S(2)}) copy-start(f32[704,128]{1,0:T(8,128)} %param.17) | copy-start | bytes 1081348
Sparse Core Ops, SparseCore 0:
  33.6 69.3 all-reduce.6
  136.4 69.4 all-reduce.4
where the time goes:
time: 225 us
  waiting for transfers between devices  139 us (62%)
  blocking collectives  63.5 us (28%)
  between operations  13.5 us (6%)
  matrix products  7.15 us (3%)
    psum x2, waiting for transfers between devices, hidden_of(): gate_sum, up_sum = lax.psum((gate_part, up_part), 'ra')  139 us
    psum x2, blocking collectives, whole_sublayer(): square_total = lax.psum(jnp.sum(as_float * as_float, axis=1), 'ra')  42.8 us
    psum x2, blocking collectives, whole_sublayer(): branch = lax.psum(branch_part, 'cb')  20.7 us
  transfers between devices with their start and end apart: 2, of which 2 were waited for; matrix products, arithmetic and copies ran while one was open for 0% of the time, Pallas kernels for 0%

commit v1 on v0

v1 whole, which is shorter than its diff:
```python
import functools

import jax
import jax.numpy as jnp
from jax import lax
from jax.experimental import pallas as pl
from jax.experimental.pallas import tpu as pltpu
from jax.sharding import PartitionSpec as P

residual_weight = 0.5
epsilon = 1e-06
MESH = pl.DeviceIdType.MESH
F32, BF16 = jnp.float32, jnp.bfloat16


def dot_t(a, b):
    return lax.dot_general(a, b, (((1,), (1,)), ((), ())), preferred_element_type=F32)


def kernel(
    n, m, x_ref, gain_a, gain_b, wg_a, wu_a, wd_a, wg_b, wu_b, wd_b, out_ref,
    wg_f, wu_f, wd_f, wg_h, wu_h, wd_h, part, slab, hslab, bslab,
    load_sem, part_send, part_recv, hid_send, hid_recv, br_send, br_recv,
):
    me = lax.axis_index("ra")
    mc = lax.axis_index("cb")
    tokens, d = x_ref.shape
    f = wg_a.shape[0]
    t = tokens // n
    width = part.shape[-1]

    barrier = pltpu.get_barrier_semaphore()
    for k in range(1, n):
        pl.semaphore_signal(
            barrier, inc=1, device_id={"ra": lax.rem(me + k, n)}, device_id_type=MESH
        )
    for k in range(1, m):
        pl.semaphore_signal(
            barrier, inc=1, device_id={"cb": lax.rem(mc + k, m)}, device_id_type=MESH
        )

    loads = {}
    for s, (g, u, w) in enumerate(((wg_a, wu_a, wd_a), (wg_b, wu_b, wd_b))):
        for j, (src, dst) in enumerate(((g, wg_f), (u, wu_f), (w, wd_f))):
            loads[s, j] = pltpu.make_async_copy(src, dst.at[s], load_sem.at[s, j])
            loads[s, j].start()

    def cast(s, j):
        src, dst = ((wg_f, wg_h), (wu_f, wu_h), (wd_f, wd_h))[j]
        loads[s, j].wait()
        dst[s] = src[s].astype(BF16)

    def part_copy(s, k):
        peer = lax.rem(me + k, n)
        return pltpu.make_async_remote_copy(
            src_ref=part.at[s, peer], dst_ref=slab.at[s, me],
            send_sem=part_send.at[s, k], recv_sem=part_recv.at[s, me],
            device_id={"ra": peer}, device_id_type=MESH,
        )

    def part_arrival(s, i):
        return pltpu.make_async_remote_copy(
            src_ref=part.at[s, i], dst_ref=slab.at[s, i],
            send_sem=part_send.at[s, 0], recv_sem=part_recv.at[s, i],
            device_id={"ra": i}, device_id_type=MESH,
        )

    def hid_copy(s, k):
        peer = lax.rem(me + k, n)
        return pltpu.make_async_remote_copy(
            src_ref=hslab.at[s, me], dst_ref=hslab.at[s, me],
            send_sem=hid_send.at[s, k], recv_sem=hid_recv.at[s, me],
            device_id={"ra": peer}, device_id_type=MESH,
        )

    def hid_arrival(s, i):
        return pltpu.make_async_remote_copy(
            src_ref=hslab.at[s, i], dst_ref=hslab.at[s, i],
            send_sem=hid_send.at[s, 0], recv_sem=hid_recv.at[s, i],
            device_id={"ra": i}, device_id_type=MESH,
        )

    def br_copy(s, k):
        peer = lax.rem(mc + k, m)
        return pltpu.make_async_remote_copy(
            src_ref=bslab.at[s, mc], dst_ref=bslab.at[s, mc],
            send_sem=br_send.at[s, k], recv_sem=br_recv.at[s, mc],
            device_id={"cb": peer}, device_id_type=MESH,
        )

    def br_arrival(s, i):
        return pltpu.make_async_remote_copy(
            src_ref=bslab.at[s, i], dst_ref=bslab.at[s, i],
            send_sem=br_send.at[s, 0], recv_sem=br_recv.at[s, i],
            device_id={"cb": i}, device_id_type=MESH,
        )

    def sublayer(s, v, gain_ref):
        square = jnp.sum(v * v, axis=1, keepdims=True)
        high = square.astype(BF16).astype(F32)
        low = square - high
        scaled = (v * gain_ref[...]).astype(BF16)
        if s == 0:
            cast(0, 0)
        gate = dot_t(scaled, wg_h[s])
        if s == 0:
            cast(0, 1)
        up = dot_t(scaled, wu_h[s])
        for j in range(n):
            rows = slice(j * t, (j + 1) * t)
            part[s, j, :, :f] = jnp.concatenate([gate[rows], up[rows]], axis=0).astype(BF16)
            part[s, j, :, f:] = jnp.broadcast_to(
                jnp.concatenate([high[rows], low[rows]], axis=0), (2 * t, width - f)
            ).astype(BF16)
        if s == 0:
            pl.semaphore_wait(barrier, n - 1 + m - 1)
        for k in range(1, n):
            part_copy(s, k).start()
        cast(s, 2)
        if s == 0:
            cast(1, 0)
            cast(1, 1)
        total = part[s, me].astype(F32)
        for k in range(1, n):
            i = lax.rem(me + k, n)
            part_arrival(s, i).wait_recv()
            total = total + slab[s, i].astype(F32)
        square_total = total[:t, f : f + 1] + total[t:, f : f + 1]
        row_scale = lax.rsqrt(square_total / (d * n) + epsilon)
        gate_sum = total[:t, :f] * row_scale
        up_sum = total[t:, :f] * row_scale
        hslab[s, me] = (gate_sum / (1.0 + jnp.exp(-gate_sum)) * up_sum).astype(BF16)
        for k in range(1, n):
            hid_copy(s, k).start()
        for k in range(1, n):
            hid_arrival(s, lax.rem(me + k, n)).wait_recv()
        hidden = jnp.concatenate([hslab[s, i].astype(F32) for i in range(n)], axis=0).astype(BF16)
        branch_part = jnp.dot(hidden, wd_h[s], preferred_element_type=F32)
        bslab[s, mc] = branch_part.astype(BF16)
        for k in range(1, m):
            br_copy(s, k).start()
        for k in range(1, m):
            br_arrival(s, lax.rem(mc + k, m)).wait_recv()
        branch = bslab[s, 0].astype(F32)
        for i in range(1, m):
            branch = branch + bslab[s, i].astype(F32)
        return (residual_weight * v + branch).astype(BF16)

    middle = sublayer(0, x_ref[...].astype(F32), gain_a)
    out_ref[...] = sublayer(1, middle.astype(F32), gain_b)

    for s in range(2):
        for k in range(1, n):
            part_copy(s, k).wait_send()
            hid_copy(s, k).wait_send()
        for k in range(1, m):
            br_copy(s, k).wait_send()


def solution(mesh):
    n, m = mesh.shape["ra"], mesh.shape["cb"]

    def per_device(tokens, ga, wg_a, wu_a, wd_a, gb, wg_b, wu_b, wd_b):
        rows, d = tokens.shape
        f = wg_a.shape[1]
        t = rows // n
        width = (f // 128 + 1) * 128
        vmem = pl.BlockSpec(memory_space=pltpu.VMEM)
        hbm = pl.BlockSpec(memory_space=pltpu.HBM)
        dma = pltpu.SemaphoreType.DMA
        return pl.pallas_call(
            functools.partial(kernel, n, m),
            out_shape=jax.ShapeDtypeStruct((rows, d), BF16),
            in_specs=[vmem] * 3 + [hbm] * 6,
            out_specs=vmem,
            scratch_shapes=[
                pltpu.VMEM((2, f, d), F32),
                pltpu.VMEM((2, f, d), F32),
                pltpu.VMEM((2, f, d), F32),
                pltpu.VMEM((2, f, d), BF16),
                pltpu.VMEM((2, f, d), BF16),
                pltpu.VMEM((2, f, d), BF16),
                pltpu.VMEM((2, n, 2 * t, width), BF16),
                pltpu.VMEM((2, n, 2 * t, width), BF16),
                pltpu.VMEM((2, n, t, f), BF16),
                pltpu.VMEM((2, m, rows, d), BF16),
                dma((2, 3)),
                dma((2, n)), dma((2, n)), dma((2, n)), dma((2, n)), dma((2, m)), dma((2, m)),
            ],
            compiler_params=pltpu.CompilerParams(collective_id=0, has_side_effects=True),
        )(tokens, ga.reshape(1, d), gb.reshape(1, d), wg_a.T, wu_a.T, wd_a, wg_b.T, wu_b.T, wd_b)

    weights = (P("ra", "cb"), P("ra", "cb"), P("cb", "ra"))
    placed = (P(None, "ra"), P("ra")) + weights + (P("ra"),) + weights
    return jax.shard_map(
        per_device, mesh=mesh, in_specs=placed, out_specs=P(None, "ra"), check_vma=False
    )
```

time: 225 us -> 39.2 us (0.17)
  waiting for transfers between devices: 139 us -> 0 us
  blocking collectives: 63.5 us -> 0 us
  Pallas kernels: 0 us -> 37.6 us
  between operations: 13.5 us -> 0.01 us
  matrix products: 7.15 us -> 0 us
    psum x2 -> x0, waiting for transfers between devices: 139 us -> none  [hidden_of(): gate_sum, up_sum = lax.psum((gate_part, up_part), 'ra')]
    psum x4 -> x0, blocking collectives: 63.5 us -> none  [the longest x2 42.8 us: whole_sublayer(): square_total = lax.psum(jnp.sum(as_float * as_float, axis=1), 'ra')]
    pallas_call x0 -> x1, Pallas kernels: none -> 37.6 us  [per_device(): pl.pallas_call(functools.partial(kernel, n, m), out_shape=jax.ShapeDtypeS...]
    dot_general x6 -> x0, matrix products: 7.15 us -> none  [the longest x2 2.85 us: hidden_of(): up_part = jnp.dot(normed, up_cast, preferred_element_type=jnp.float32)]
  transfers between devices with their start and end apart: 2 -> 0, of which waited for: 2 -> 0; matrix products, arithmetic and copies ran while one was open for 0% -> 0% of each run, Pallas kernels for 0% -> 0%
where the time goes in v1:
time: 39.2 us; the launch traced here: 39 us
  Pallas kernels  37.6 us (96%)
  local copies, waits for them, and re-layouts  1.32 us (3%)
    pallas_call x1, Pallas kernels, per_device(): pl.pallas_call(functools.partial(kernel, n, m), out_shape=jax.ShapeDtypeS...  37.6 us
    unnamed x1, local copies, waits for them, and re-layouts  1.32 us

profile of v1, /device:TPU:0, one launch (start us, length us, event | category | flops | bytes accessed | tf_op | source)
XLA Modules:
  0.0 39.0 jit_solution(17308471882938268835)
XLA Ops:
  0.0 37.6 %shard_map.91 = bf16[64,128]{1,0:T(8,128)(2,1)} custom-call(bf16[64,128]{1,0:T(8,128)(2,1)} %x_ref.1, f32[1,128]{1,0:T(1,128)} %bitcast.10, f32[1,128]{1,0:T(1,128)} %bitcast.11, f32[704,128]{1,0:T(8,128)} %bitcast.6, f32[704,128]{1,0:T(8,128)} %bitcast.7, f32[704,128]{1,0:T(8,128)} %wd_a.1, f32[704,128]{1,0:T(8,128)} %bitcast.8, f32[704,128]{1,0:T(8,128)} %bitcast.9, ...), custom_call_target="tpu_custom_call" | custom-call | tf_op jit(solution)/shard_map/pallas_call | solution.py:171
  37.6 1.3 %copy.11 = bf16[64,128]{1,0:T(8,128)(2,1)} copy(bf16[64,128]{1,0:T(8,128)(2,1)} %shard_map.91) | data formatting | bytes 32768

commit v2 on v1

v2 whole, which is shorter than its diff:
```python
import functools

import jax
import jax.numpy as jnp
from jax import lax
from jax.experimental import pallas as pl
from jax.experimental.pallas import tpu as pltpu
from jax.sharding import PartitionSpec as P

residual_weight = 0.5
epsilon = 1e-06
CHAINS = 1
MESH = pl.DeviceIdType.MESH
F32, BF16 = jnp.float32, jnp.bfloat16


def dot_t(a, b):
    return lax.dot_general(a, b, (((1,), (1,)), ((), ())), preferred_element_type=F32)


def partner(me, k, n):
    if n & (n - 1):
        return lax.rem(me + k, n)
    peer, bit = me, 1
    while bit < n:
        if k & bit:
            peer = peer + bit - 2 * bit * ((me // bit) % 2)
        bit *= 2
    return peer


def giver(me, k, n):
    return lax.rem(me + n - k, n) if n & (n - 1) else partner(me, k, n)


def kernel(
    n, m, chains, x_in, gain_a, gain_b, wg_a, wu_a, wd_a, wg_b, wu_b, wd_b, out_ref,
    x_ref, gains, wg_f, wu_f, wd_f, wg_h, wu_h, wd_h, part, slab, hslab, bslab,
    load_sem, small_sem, part_send, part_recv, hid_send, hid_recv, br_send, br_recv,
):
    me = lax.axis_index("ra")
    mc = lax.axis_index("cb")
    tokens, d = x_in.shape
    f = wg_a.shape[0]
    rows = tokens // chains
    t = rows // n
    width = part.shape[-1]
    far = range(n - 1, 0, -1)
    wide = range(m - 1, 0, -1)

    barrier = pltpu.get_barrier_semaphore()
    for k in far:
        pl.semaphore_signal(
            barrier, inc=1, device_id={"ra": partner(me, k, n)}, device_id_type=MESH
        )
    for k in wide:
        pl.semaphore_signal(
            barrier, inc=1, device_id={"cb": partner(mc, k, m)}, device_id_type=MESH
        )

    small = [
        pltpu.make_async_copy(x_in, x_ref, small_sem.at[0]),
        pltpu.make_async_copy(gain_a, gains.at[0], small_sem.at[1]),
        pltpu.make_async_copy(gain_b, gains.at[1], small_sem.at[2]),
    ]
    for copy in small:
        copy.start()
    loads = {}
    for s, (g, u, w) in enumerate(((wg_a, wu_a, wd_a), (wg_b, wu_b, wd_b))):
        for j, (src, dst) in enumerate(((g, wg_f), (u, wu_f), (w, wd_f))):
            loads[s, j] = pltpu.make_async_copy(src, dst.at[s], load_sem.at[s, j])
            loads[s, j].start()

    def cast(s, j):
        src, dst = ((wg_f, wg_h), (wu_f, wu_h), (wd_f, wd_h))[j]
        loads[s, j].wait()
        dst[s] = src[s].astype(BF16)

    def remote(src, dst, send, recv, axis, peer):
        return pltpu.make_async_remote_copy(
            src_ref=src, dst_ref=dst, send_sem=send, recv_sem=recv,
            device_id={axis: peer}, device_id_type=MESH,
        )

    def part_copy(s, q, k):
        peer = partner(me, k, n)
        return remote(
            part.at[s, q, peer], slab.at[s, q, k], part_send.at[s, q, k], part_recv.at[s, q, k],
            "ra", peer,
        )

    def hid_copy(s, q, k, owner, peer):
        block = hslab.at[s, q, owner]
        return remote(block, block, hid_send.at[s, q, k], hid_recv.at[s, q, k], "ra", peer)

    def br_copy(s, q, k, owner, peer):
        block = bslab.at[s, q, owner]
        return remote(block, block, br_send.at[s, q, k], br_recv.at[s, q, k], "cb", peer)

    def project(s, q, v):
        square = jnp.sum(v * v, axis=1, keepdims=True)
        high = square.astype(BF16).astype(F32)
        low = square - high
        scaled = (v * gains[s]).astype(BF16)
        if s == 0 and q == 0:
            cast(0, 0)
            cast(0, 1)
        gate = dot_t(scaled, wg_h[s])
        up = dot_t(scaled, wu_h[s])
        for j in range(n):
            own = slice(j * t, (j + 1) * t)
            part[s, q, j, :, :f] = jnp.concatenate([gate[own], up[own]], axis=0).astype(BF16)
            part[s, q, j, :, f:] = jnp.broadcast_to(
                jnp.concatenate([high[own], low[own]], axis=0), (2 * t, width - f)
            ).astype(BF16)
        if s == 0 and q == 0:
            pl.semaphore_wait(barrier, n - 1 + m - 1)
        for k in far:
            part_copy(s, q, k).start()

    def activate(s, q):
        total = part[s, q, me].astype(F32)
        for k in far:
            part_copy(s, q, k).wait_recv()
            total = total + slab[s, q, k].astype(F32)
        square_total = total[:t, f : f + 1] + total[t:, f : f + 1]
        row_scale = lax.rsqrt(square_total / (d * n) + epsilon)
        gate_sum = total[:t, :f] * row_scale
        up_sum = total[t:, :f] * row_scale
        hslab[s, q, me] = (gate_sum / (1.0 + jnp.exp(-gate_sum)) * up_sum).astype(BF16)
        for k in far:
            hid_copy(s, q, k, me, partner(me, k, n)).start()

    def contract(s, q):
        for k in far:
            i = giver(me, k, n)
            hid_copy(s, q, k, i, i).wait_recv()
        hidden = jnp.concatenate([hslab[s, q, i].astype(F32) for i in range(n)], axis=0)
        branch_part = jnp.dot(hidden.astype(BF16), wd_h[s], preferred_element_type=F32)
        bslab[s, q, mc] = branch_part.astype(BF16)
        for k in wide:
            br_copy(s, q, k, mc, partner(mc, k, m)).start()

    def finish(s, q, v):
        for k in wide:
            i = giver(mc, k, m)
            br_copy(s, q, k, i, i).wait_recv()
        branch = bslab[s, q, 0].astype(F32)
        for i in range(1, m):
            branch = branch + bslab[s, q, i].astype(F32)
        return (residual_weight * v + branch).astype(BF16)

    for copy in small:
        copy.wait()
    streams = [x_ref[q * rows : (q + 1) * rows].astype(F32) for q in range(chains)]
    for q in range(chains):
        project(0, q, streams[q])
    cast(0, 2)
    for j in range(3):
        cast(1, j)
    for s in range(2):
        for q in range(chains):
            activate(s, q)
        for q in range(chains):
            contract(s, q)
        for q in range(chains):
            done = finish(s, q, streams[q])
            if s == 0:
                streams[q] = done.astype(F32)
                project(1, q, streams[q])
            else:
                out_ref[q * rows : (q + 1) * rows] = done

    for s in range(2):
        for q in range(chains):
            for k in far:
                part_copy(s, q, k).wait_send()
                hid_copy(s, q, k, me, partner(me, k, n)).wait_send()
            for k in wide:
                br_copy(s, q, k, mc, partner(mc, k, m)).wait_send()


def solution(mesh):
    n, m = mesh.shape["ra"], mesh.shape["cb"]

    def per_device(tokens, ga, wg_a, wu_a, wd_a, gb, wg_b, wu_b, wd_b):
        rows, d = tokens.shape
        f = wg_a.shape[1]
        chains = CHAINS if rows % (CHAINS * n) == 0 else 1
        t = rows // (n * chains)
        width = (f // 128 + 1) * 128
        vmem = pl.BlockSpec(memory_space=pltpu.VMEM)
        hbm = pl.BlockSpec(memory_space=pltpu.HBM)
        dma = pltpu.SemaphoreType.DMA
        return pl.pallas_call(
            functools.partial(kernel, n, m, chains),
            out_shape=jax.ShapeDtypeStruct((rows, d), BF16),
            in_specs=[hbm] * 9,
            out_specs=vmem,
            scratch_shapes=[
                pltpu.VMEM((rows, d), BF16),
                pltpu.VMEM((2, 1, d), F32),
                pltpu.VMEM((2, f, d), F32),
                pltpu.VMEM((2, f, d), F32),
                pltpu.VMEM((2, f, d), F32),
                pltpu.VMEM((2, f, d), BF16),
                pltpu.VMEM((2, f, d), BF16),
                pltpu.VMEM((2, f, d), BF16),
                pltpu.VMEM((2, chains, n, 2 * t, width), BF16),
                pltpu.VMEM((2, chains, n, 2 * t, width), BF16),
                pltpu.VMEM((2, chains, n, t, f), BF16),
                pltpu.VMEM((2, chains, m, rows // chains, d), BF16),
                dma((2, 3)), dma((3,)),
                dma((2, chains, n)), dma((2, chains, n)), dma((2, chains, n)),
                dma((2, chains, n)), dma((2, chains, m)), dma((2, chains, m)),
            ],
            compiler_params=pltpu.CompilerParams(collective_id=0, has_side_effects=True),
        )(tokens, ga.reshape(1, d), gb.reshape(1, d), wg_a.T, wu_a.T, wd_a, wg_b.T, wu_b.T, wd_b)

    weights = (P("ra", "cb"), P("ra", "cb"), P("cb", "ra"))
    placed = (P(None, "ra"), P("ra")) + weights + (P("ra"),) + weights
    return jax.shard_map(
        per_device, mesh=mesh, in_specs=placed, out_specs=P(None, "ra"), check_vma=False
    )
```

time: 39.2 us -> 35.9 us (0.916)
  Pallas kernels: 37.6 us -> 34.3 us
    pallas_call x1, Pallas kernels: 37.6 us -> 34.3 us  [per_device(): pl.pallas_call(functools.partial(kernel, n, m, chains), out_shape=jax.Sha...]
where the time goes in v2:
time: 35.9 us; the launch traced here: 35.6 us
  Pallas kernels  34.3 us (96%)
  local copies, waits for them, and re-layouts  1.32 us (4%)
    pallas_call x1, Pallas kernels, per_device(): pl.pallas_call(functools.partial(kernel, n, m, chains), out_shape=jax.Sha...  34.3 us
    unnamed x1, local copies, waits for them, and re-layouts  1.32 us

profile of v2, /device:TPU:0, one launch (start us, length us, event | category | flops | bytes accessed | tf_op | source)
XLA Modules:
  0.0 35.6 jit_solution(9518386430045670316)
XLA Ops:
  0.0 34.3 %shard_map.91 = bf16[64,128]{1,0:T(8,128)(2,1)} custom-call(bf16[64,128]{1,0:T(8,128)(2,1)} %x_in.1, f32[1,128]{1,0:T(1,128)} %bitcast.10, f32[1,128]{1,0:T(1,128)} %bitcast.11, f32[704,128]{1,0:T(8,128)} %bitcast.6, f32[704,128]{1,0:T(8,128)} %bitcast.7, f32[704,128]{1,0:T(8,128)} %wd_a.1, f32[704,128]{1,0:T(8,128)} %bitcast.8, f32[704,128]{1,0:T(8,128)} %bitcast.9, ...), custom_call_target="tpu_custom_call" | custom-call | tf_op jit(solution)/shard_map/pallas_call | solution.py:195
  34.3 1.3 %copy.11 = bf16[64,128]{1,0:T(8,128)(2,1)} copy(bf16[64,128]{1,0:T(8,128)(2,1)} %shard_map.91) | data formatting | bytes 32768

commit v3 on v2

--- a/solution.py
+++ b/solution.py
@@ -10,6 +10,7 @@
 residual_weight = 0.5
 epsilon = 1e-06
 CHAINS = 1
+VMEM_LIMIT = 56518246
 MESH = pl.DeviceIdType.MESH
 F32, BF16 = jnp.float32, jnp.bfloat16
 
@@ -27,6 +28,13 @@
             peer = peer + bit - 2 * bit * ((me // bit) % 2)
         bit *= 2
     return peer
+
+
+def send_order(n):
+    if n % 2:
+        return list(range(n - 1, 0, -1))
+    pairs = sorted(range(1, n // 2), key=lambda z: (abs(z - n // 4), -z))
+    return [2 * z + 1 for z in pairs] + [2 * z for z in pairs] + [1]
 
 
 def giver(me, k, n):
@@ -45,7 +53,7 @@
     rows = tokens // chains
     t = rows // n
     width = part.shape[-1]
-    far = range(n - 1, 0, -1)
+    far = send_order(n)
     wide = range(m - 1, 0, -1)
 
     barrier = pltpu.get_barrier_semaphore()
@@ -214,7 +222,7 @@
                 dma((2, chains, n)), dma((2, chains, n)), dma((2, chains, n)),
                 dma((2, chains, n)), dma((2, chains, m)), dma((2, chains, m)),
             ],
-            compiler_params=pltpu.CompilerParams(collective_id=0, has_side_effects=True),
+            compiler_params=pltpu.CompilerParams(collective_id=0, has_side_effects=True, vmem_limit_bytes=VMEM_LIMIT),
         )(tokens, ga.reshape(1, d), gb.reshape(1, d), wg_a.T, wu_a.T, wd_a, wg_b.T, wu_b.T, wd_b)
 
     weights = (P("ra", "cb"), P("ra", "cb"), P("cb", "ra"))

time: 35.9 us -> 34.2 us (0.953)
  Pallas kernels: 34.3 us -> 32.7 us
    pallas_call x1, Pallas kernels: 34.3 us -> 32.7 us  [per_device(): pl.pallas_call(functools.partial(kernel, n, m, chains), out_shape=jax.Sha...]
    unnamed x1 -> x5, local copies, waits for them, and re-layouts: 1.32 us -> 1.28 us
where the time goes in v3:
time: 34.2 us; the launch traced here: 34 us
  Pallas kernels  32.7 us (96%)
  local copies, waits for them, and re-layouts  1.28 us (4%)
    pallas_call x1, Pallas kernels, per_device(): pl.pallas_call(functools.partial(kernel, n, m, chains), out_shape=jax.Sha...  32.7 us
    unnamed x5, local copies, waits for them, and re-layouts  1.28 us

profile of v3, /device:TPU:0, one launch (start us, length us, event | category | flops | bytes accessed | tf_op | source)
XLA Modules:
  0.0 34.0 jit_solution(10043807852995430938)
XLA Ops:
  0.0 0.0 copy-start
  0.0 0.0 copy-start.1
  0.0 0.7 %copy-done = f32[128]{0:T(128)S(1)} copy-done((f32[128]{0:T(128)S(1)}, f32[128]{0:T(128)}, u32[]{:S(2)}) %copy-start) | copy-done | bytes 536
  0.7 0.0 copy-done.1
  0.7 32.7 %shard_map.91 = bf16[64,128]{1,0:T(8,128)(2,1)S(1)} custom-call(bf16[64,128]{1,0:T(8,128)(2,1)} %x_in.1, f32[1,128]{1,0:T(1,128)S(1)} %bitcast.6, f32[1,128]{1,0:T(1,128)S(1)} %bitcast.7, f32[704,128]{1,0:T(8,128)} %bitcast.8, f32[704,128]{1,0:T(8,128)} %bitcast.9, f32[704,128]{1,0:T(8,128)} %wd_a.1, f32[704,128]{1,0:T(8,128)} %bitcast.10, ...), custom_call_target="tpu_custom_call" | custom-call | tf_op jit(solution)/shard_map/pallas_call | solution.py:203
  33.4 0.6 %copy.11 = bf16[64,128]{1,0:T(8,128)(2,1)} copy(bf16[64,128]{1,0:T(8,128)(2,1)S(1)} %shard_map.91) | data formatting | bytes 32768
Async XLA Ops:
  0.0 0.7 %copy-start = (f32[128]{0:T(128)S(1)}, f32[128]{0:T(128)}, u32[]{:S(2)}) copy-start(f32[128]{0:T(128)} %param.10) | copy-start | bytes 1540
  0.0 0.7 %copy-start.1 = (f32[128]{0:T(128)S(1)}, f32[128]{0:T(128)}, u32[]{:S(2)}) copy-start(f32[128]{0:T(128)} %param.14) | copy-start | bytes 1540

commit v4 on v3

--- a/solution.py
+++ b/solution.py
@@ -143,8 +143,8 @@
         for k in far:
             i = giver(me, k, n)
             hid_copy(s, q, k, i, i).wait_recv()
-        hidden = jnp.concatenate([hslab[s, q, i].astype(F32) for i in range(n)], axis=0)
-        branch_part = jnp.dot(hidden.astype(BF16), wd_h[s], preferred_element_type=F32)
+        hidden = jnp.concatenate([hslab[s, q, i] for i in range(n)], axis=0)
+        branch_part = jnp.dot(hidden, wd_h[s], preferred_element_type=F32)
         bslab[s, q, mc] = branch_part.astype(BF16)
         for k in wide:
             br_copy(s, q, k, mc, partner(mc, k, m)).start()

time: 34.2 us -> 34.2 us (level)
  no operation moved by 1% of the time
where the time goes in v4:
time: 34.2 us; the launch traced here: 34 us
  Pallas kernels  32.7 us (96%)
  local copies, waits for them, and re-layouts  1.28 us (4%)
    pallas_call x1, Pallas kernels, per_device(): pl.pallas_call(functools.partial(kernel, n, m, chains), out_shape=jax.Sha...  32.7 us
    unnamed x5, local copies, waits for them, and re-layouts  1.28 us

profile of v4, /device:TPU:0, one launch (start us, length us, event | category | flops | bytes accessed | tf_op | source)
XLA Modules:
  0.0 34.0 jit_solution(16655960660962223791)
XLA Ops:
  0.0 0.0 copy-start
  0.0 0.0 copy-start.1
  0.0 0.7 %copy-done = f32[128]{0:T(128)S(1)} copy-done((f32[128]{0:T(128)S(1)}, f32[128]{0:T(128)}, u32[]{:S(2)}) %copy-start) | copy-done | bytes 536
  0.7 0.0 copy-done.1
  0.7 32.7 %shard_map.91 = bf16[64,128]{1,0:T(8,128)(2,1)S(1)} custom-call(bf16[64,128]{1,0:T(8,128)(2,1)} %x_in.1, f32[1,128]{1,0:T(1,128)S(1)} %bitcast.6, f32[1,128]{1,0:T(1,128)S(1)} %bitcast.7, f32[704,128]{1,0:T(8,128)} %bitcast.8, f32[704,128]{1,0:T(8,128)} %bitcast.9, f32[704,128]{1,0:T(8,128)} %wd_a.1, f32[704,128]{1,0:T(8,128)} %bitcast.10, ...), custom_call_target="tpu_custom_call" | custom-call | tf_op jit(solution)/shard_map/pallas_call | solution.py:203
  33.4 0.6 %copy.11 = bf16[64,128]{1,0:T(8,128)(2,1)} copy(bf16[64,128]{1,0:T(8,128)(2,1)S(1)} %shard_map.91) | data formatting | bytes 32768
Async XLA Ops:
  0.0 0.7 %copy-start = (f32[128]{0:T(128)S(1)}, f32[128]{0:T(128)}, u32[]{:S(2)}) copy-start(f32[128]{0:T(128)} %param.10) | copy-start | bytes 1540
  0.0 0.7 %copy-start.1 = (f32[128]{0:T(128)S(1)}, f32[128]{0:T(128)}, u32[]{:S(2)}) copy-start(f32[128]{0:T(128)} %param.14) | copy-start | bytes 1540
